TPU v7x, 32 devices: a whole 2x2x4 slice. The times are simulated.
32 devices in a mesh: ep: 4 (over z), tp: 8 (over y, x, core).
Axes of the slice: x: 2, y: 2, z: 4, core: 2. Of those that a mesh axis runs over, the one named last changes fastest.
Arguments:
- hidden: bfloat16 [64, 4096], P('ep', 'tp'), may hold values from -6 to 6
- norm_gain: float32 [4096], replicated, may hold values from 0.1 to 1.9
- routes: int32 [64, 4], P('ep'), may hold values from 0 to 7, all different within a row; in each aligned block of 16 rows (0 to 15, 16 to 31, ...) at most 13 rows name the same one
- route_weights: float32 [64, 4], P('ep'), may hold values from 0.1 to 1
- gate_weight: bfloat16 [8, 1024, 4096], P('ep', 'tp'), may hold values from -0.09375 to 0.09375
- up_weight: bfloat16 [8, 1024, 4096], P('ep', 'tp'), may hold values from -0.09375 to 0.09375
- down_weight: bfloat16 [8, 1024, 4096], P('ep', 'tp'), may hold values from -0.25 to 0.25
- shared_gate: bfloat16 [1024, 4096], P('tp'), may hold values from -0.09375 to 0.09375
- shared_up: bfloat16 [1024, 4096], P('tp'), may hold values from -0.09375 to 0.09375
- shared_down: bfloat16 [1024, 4096], P('tp'), may hold values from -0.25 to 0.25
Outputs:
- mixed: bfloat16 [64, 4096], P('ep', 'tp')
Inputs may be any that keep to these rules, and one draw needn't show every extreme that they name: `routes`: each row names 4 different experts; among the rows of one index of ep (aligned blocks of 16 rows) no expert is named more than 13 times, a bound that some block reaches.
All inputs are finite; a program needn't handle non-finite values.
Results may differ from a plain program's by a relative error of at most 0.017.
Values may be sent and summed in bfloat16 or wider, within the bound.
A program may use at most 64 MiB of HBM per device.

v0:
```python
import jax
import jax.numpy as jnp
from jax import lax
from jax.sharding import PartitionSpec as P

norm_eps = 1e-06


def norm_rows(gathered, norm_gain):
    values = gathered.astype(jnp.float32)
    inv_scale = lax.rsqrt(jnp.mean(values * values, axis=-1, keepdims=True) + norm_eps)
    return (values * inv_scale * norm_gain).astype(jnp.bfloat16)


def slot_table(routes, expert_count, capacity):
    onehot = (
        routes[:, :, None] == jnp.arange(expert_count, dtype=jnp.int32)[None, None, :]
    ).astype(jnp.int32)
    used_mask = jnp.sum(onehot, axis=1)
    before = jnp.cumsum(used_mask, axis=0) - used_mask
    slot_rank = jnp.sum(onehot * before[:, None, :], axis=2)
    return routes * capacity + slot_rank


def per_device(
    hidden,
    norm_gain,
    routes,
    route_weights,
    gate_weight,
    up_weight,
    down_weight,
    shared_gate,
    shared_up,
    shared_down,
):
    width_group = lax.axis_size("tp")
    down_local = lax.all_to_all(down_weight, "tp", split_axis=2, concat_axis=1, tiled=True)
    gathered = lax.all_gather(hidden, "tp", axis=1, tiled=True)
    normed = norm_rows(gathered, norm_gain)
    tok_rows, top_count = routes.shape
    local_experts = gate_weight.shape[0]
    groups = lax.axis_size("ep")
    experts = local_experts * groups
    capacity = min(tok_rows, 3 * tok_rows * top_count // (2 * experts) + 1)
    full_width = gathered.shape[1]
    slot_ids = slot_table(routes, experts, capacity)
    slot_range = jnp.arange(experts * capacity, dtype=jnp.int32)
    matches = slot_ids[:, :, None] == slot_range[None, None, :]
    combine = jnp.sum(jnp.where(matches, route_weights[:, :, None], 0.0), axis=1)
    select = jnp.sum(
        (slot_range[:, None, None] == slot_ids[None, :, :]).astype(jnp.bfloat16), axis=2
    )
    packed = jnp.dot(select, normed, preferred_element_type=jnp.float32).astype(jnp.bfloat16)
    packed = packed.reshape(groups, local_experts, capacity, full_width)
    arrived = lax.all_to_all(packed, "ep", split_axis=0, concat_axis=0, tiled=True)
    gate_vals = jnp.einsum(
        "secd,efd->secf", arrived, gate_weight, preferred_element_type=jnp.float32
    )
    up_vals = jnp.einsum("secd,efd->secf", arrived, up_weight, preferred_element_type=jnp.float32)
    inner_vals = (jax.nn.silu(gate_vals) * up_vals).astype(jnp.bfloat16)
    dims = (((1,), (1,)), ((), ()))
    shared_gates = lax.dot_general(normed, shared_gate, dims, preferred_element_type=jnp.float32)
    shared_ups = lax.dot_general(normed, shared_up, dims, preferred_element_type=jnp.float32)
    shared_inner = (jax.nn.silu(shared_gates) * shared_ups).astype(jnp.bfloat16)
    shared_part = jnp.dot(shared_inner, shared_down, preferred_element_type=jnp.float32).astype(
        jnp.bfloat16
    )
    inner_whole = lax.all_gather(inner_vals, "tp", axis=3, tiled=True)
    slots, _, cap_rows, hidden_units = inner_whole.shape
    block_units = hidden_units // width_group
    inner_blocks = inner_whole.reshape(slots, local_experts, cap_rows, width_group, block_units)
    down_blocks = down_local.reshape(local_experts, width_group, block_units, down_local.shape[2])
    block_sums = jnp.einsum(
        "secpf,epfd->secpd", inner_blocks, down_blocks, preferred_element_type=jnp.float32
    ).astype(jnp.bfloat16)
    answers = jnp.sum(block_sums.astype(jnp.float32), axis=3).astype(jnp.bfloat16)
    shared_sum = lax.psum_scatter(shared_part, "tp", scatter_dimension=1, tiled=True).astype(
        jnp.float32
    )
    returned = lax.all_to_all(answers, "ep", split_axis=0, concat_axis=0, tiled=True)
    flat_rows = returned.reshape(-1, returned.shape[3]).astype(jnp.float32)
    routed = jnp.dot(combine, flat_rows, precision=lax.Precision.HIGHEST)
    return (routed + shared_sum).astype(jnp.bfloat16)


def solution(mesh):
    in_specs = (
        P("ep", "tp"),
        P(),
        P("ep", None),
        P("ep", None),
        P("ep", "tp", None),
        P("ep", "tp", None),
        P("ep", "tp", None),
        P("tp", None),
        P("tp", None),
        P("tp", None),
    )
    out_specs = P("ep", "tp")
    return jax.shard_map(
        per_device, mesh=mesh, in_specs=in_specs, out_specs=out_specs, check_vma=False
    )
```

profile of v0, /device:TPU:0, one launch (start us, length us, event | category | flops | bytes accessed | tf_op | source)
XLA Modules:
  0.0 113.9 jit_solution(8584589679115222297)
XLA Ops:
  6.5 0.8 convert_reduce_fusion
  7.4 0.1 copy.40
  7.5 0.1 copy.42
  7.6 0.7 select_reduce_fusion.1
  8.3 0.7 multiply_add_fusion
  9.0 0.1 fusion.33
  9.0 10.9 %all_gather.6 = bf16[16,4096]{1,0:T(8,128)(2,1)S(1)} all-gather(bf16[16,512]{1,0:T(8,128)(2,1)} %param.10), channel_id=1, replica_groups=mesh['ep'=4,'tp'=8] {'tp'}, dimensions={1}, use_global_device_ids=true | all-gather | bytes 147456 | tf_op jit(solution)/shard_map/all_gather | solution.py:39
  19.9 0.1 fusion.28
  20.1 2.1 %convolution_convert_fusion = bf16[104,4096]{1,0:T(8,128)(2,1)} fusion(bf16[104,16]{0,1:T(8,128)(2,1)S(1)} %fusion.33, bf16[16,4096]{1,0:T(8,128)(2,1)S(1)} %all_gather.6, f32[4096]{0:T(1024)} %param.11, f32[16]{0:T(128)S(1)} %add_rsqrt_fusion), kind=kOutput, calls=%fused_computation | convolution fusion | flops 14319616 | bytes 1002816 | tf_op jit(solution)/shard_map/dot_general | solution.py:54
  22.2 1.4 %reshape.33 = bf16[4,2,13,4096]{3,2,1,0:T(8,128)(2,1)S(1)} reshape(bf16[104,4096]{1,0:T(8,128)(2,1)} %convolution_convert_fusion) | data formatting | bytes 1703936 | tf_op jit(solution)/shard_map/reshape | solution.py:55
  23.6 1.8 %copy.43 = bf16[4,2,13,4096]{3,1,2,0:T(2,128)(2,1)} copy(bf16[4,2,13,4096]{3,2,1,0:T(8,128)(2,1)S(1)} %reshape.33) | data formatting | bytes 1703936 | tf_op jit(solution)/shard_map/reshape | solution.py:55
  25.4 4.9 %all-to-all-start = ((bf16[4,2,13,4096]{3,1,2,0:T(2,128)(2,1)}), bf16[4,2,13,4096]{3,1,2,0:T(2,128)(2,1)S(1)}, u32[]{:S(2)}, u32[]{:S(2)}) async-start(bf16[4,2,13,4096]{3,1,2,0:T(2,128)(2,1)} %copy.43), calls=%async_computation | async-start | bytes 1703936 | tf_op jit(solution)/shard_map/all_to_all | solution.py:56
  30.3 6.2 %copy.47 = bf16[2,128,4096]{1,0,2:T(2,128)(2,1)} copy(bf16[2,128,4096]{2,1,0:T(8,128)(2,1)} %param.16) | data formatting | bytes 4194304 | tf_op args[6]
  36.5 15.8 %all-to-all-done = bf16[4,2,13,4096]{3,1,2,0:T(2,128)(2,1)S(1)} async-done(((bf16[4,2,13,4096]{3,1,2,0:T(2,128)(2,1)}), bf16[4,2,13,4096]{3,1,2,0:T(2,128)(2,1)S(1)}, u32[]{:S(2)}, u32[]{:S(2)}) %all-to-all-start) | async-done | bytes 852000 | tf_op jit(solution)/shard_map/all_to_all | solution.py:56
  52.3 4.3 %all-to-all-start.1 = ((bf16[2,128,4096]{1,0,2:T(2,128)(2,1)}), bf16[2,128,4096]{1,0,2:T(2,128)(2,1)}, u32[]{:S(2)}, u32[]{:S(2)}) async-start(bf16[2,128,4096]{1,0,2:T(2,128)(2,1)} %copy.47), calls=%async_computation.1 | async-start | bytes 4194304 | tf_op jit(solution)/shard_map/all_to_all | solution.py:38
  56.7 0.0 reduce-scatter.2.cloned.1.call-start
  56.7 1.6 %fusion.43 = f32[16,128]{1,0:T(8,128)S(1)} fusion(bf16[128,4096]{1,0:T(8,128)(2,1)} %param.17, bf16[16,4096]{1,0:T(8,128)(2,1)S(1)} %all_gather.6, f32[4096]{0:T(1024)S(1)} %copy-done.2, f32[16]{0:T(128)S(1)} %add_rsqrt_fusion), kind=kOutput, calls=%fused_computation.43 | convolution fusion | flops 17039360 | bytes 1204288 | tf_op jit(solution)/shard_map/dot_general | solution.py:63
  58.4 3.1 %convolution_convert_fusion.1 = bf16[16,4096]{1,0:T(8,128)(2,1)} fusion(bf16[128,4096]{1,0:T(8,128)(2,1)} %param.19, bf16[128,4096]{1,0:T(8,128)(2,1)} %param.18, f32[16,128]{1,0:T(8,128)S(1)} %fusion.43, bf16[16,4096]{1,0:T(8,128)(2,1)S(1)} %all_gather.6, f32[4096]{0:T(1024)S(1)} %copy-done.2, f32[16]{0:T(128)S(1)} %add_rsqrt_fusion), kind=kOutput, calls=%fused_computation.1 | convolution fusion | flops 33894400 | bytes 2383936 | tf_op jit(solution)/shard_map/dot_general | solution.py:66
  61.6 0.8 fusion.12
  62.4 0.7 copy-done.1
  63.1 0.9 fusion.21
  64.0 22.9 %all_gather.7 = bf16[4,2,13,1024]{3,2,0,1:T(8,128)(2,1)S(1)} all-gather(bf16[4,2,13,128]{3,2,0,1:T(8,128)(2,1)S(1)} %fusion.21), channel_id=1, replica_groups=mesh['ep'=4,'tp'=8] {'tp'}, dimensions={3}, use_global_device_ids=true | all-gather | bytes 239616 | tf_op jit(solution)/shard_map/all_gather | solution.py:69
  86.9 0.2 reshape.39
  87.1 6.2 %copy.49 = bf16[2,128,8,512]{3,1,2,0:T(8,128)(2,1)} copy(bf16[2,128,8,512]{1,0,3,2:T(2,128)(2,1)} %bitcast.6) | data formatting | bytes 4194304 | tf_op jit(solution)/shard_map/all_to_all | solution.py:38
  93.2 2.1 %fusion.9 = bf16[2,4,13,512]{3,2,1,0:T(8,128)(2,1)S(1)} fusion(bf16[2,128,8,512]{3,1,2,0:T(8,128)(2,1)} %copy.49, bf16[4,2,13,8,128]{4,3,2,0,1:T(8,128)(2,1)S(1)} %reshape.39), kind=kOutput, calls=%fused_computation.9 | convolution fusion | flops 109850624 | bytes 2416640 | tf_op jit(solution)/shard_map/secpf,epfd->secpd/dot_general | solution.py:74
  95.3 0.8 copy.51
  96.1 3.3 %all-to-all-start.2 = ((bf16[4,2,13,512]{3,1,2,0:T(2,128)(2,1)}), bf16[4,2,13,512]{3,1,2,0:T(2,128)(2,1)S(1)}, u32[]{:S(2)}, u32[]{:S(2)}) async-start(bf16[4,2,13,512]{3,1,2,0:T(2,128)(2,1)} %copy.51), calls=%async_computation.2 | async-start | bytes 212992 | tf_op jit(solution)/shard_map/all_to_all | solution.py:81
  99.4 0.1 select_reduce_fusion
  99.5 6.0 %all-to-all-done.2 = bf16[4,2,13,512]{3,1,2,0:T(2,128)(2,1)S(1)} async-done(((bf16[4,2,13,512]{3,1,2,0:T(2,128)(2,1)}), bf16[4,2,13,512]{3,1,2,0:T(2,128)(2,1)S(1)}, u32[]{:S(2)}, u32[]{:S(2)}) %all-to-all-start.2) | async-done | bytes 106528 | tf_op jit(solution)/shard_map/all_to_all | solution.py:81
  105.5 0.1 reshape.35
  105.5 0.0 reduce-scatter.2.cloned.1.call-done
  105.6 1.5 %fusion.24 = bf16[16,512]{1,0:T(8,128)(2,1)} fusion(f32[16,104]{1,0:T(8,128)S(1)} %select_reduce_fusion, bf16[104,512]{1,0:T(8,128)(2,1)S(1)} %reshape.35, bf16[16,512]{1,0:T(8,128)(2,1)} %reduce-scatter.2.cloned.1.call-done), kind=kOutput, calls=%fused_computation.15 | convolution fusion | flops 10248192 | bytes 145920 | tf_op jit(solution)/shard_map/dot_general | solution.py:83
  (13 shorter events, 0.1 us)
Async XLA Ops:
  6.5 55.0 %copy-start = (bf16[2,128,4096]{2,1,0:T(8,128)(2,1)S(1)}, bf16[2,128,4096]{2,1,0:T(8,128)(2,1)}, u32[]{:S(2)}) copy-start(bf16[2,128,4096]{2,1,0:T(8,128)(2,1)} %param.14) | copy-start | bytes 6291460
  25.4 26.9 %all-to-all-start = ((bf16[4,2,13,4096]{3,1,2,0:T(2,128)(2,1)}), bf16[4,2,13,4096]{3,1,2,0:T(2,128)(2,1)S(1)}, u32[]{:S(2)}, u32[]{:S(2)}) async-start(bf16[4,2,13,4096]{3,1,2,0:T(2,128)(2,1)} %copy.43), calls=%async_computation | async-start | bytes 1703936 | tf_op jit(solution)/shard_map/all_to_all | solution.py:56
  36.5 20.2 %copy-start.2 = (f32[4096]{0:T(1024)S(1)}, f32[4096]{0:T(1024)}, u32[]{:S(2)}) copy-start(f32[4096]{0:T(1024)} %param.11) | copy-start | bytes 49156
  52.3 34.8 %all-to-all-start.1 = ((bf16[2,128,4096]{1,0,2:T(2,128)(2,1)}), bf16[2,128,4096]{1,0,2:T(2,128)(2,1)}, u32[]{:S(2)}, u32[]{:S(2)}) async-start(bf16[2,128,4096]{1,0,2:T(2,128)(2,1)} %copy.47), calls=%async_computation.1 | async-start | bytes 4194304 | tf_op jit(solution)/shard_map/all_to_all | solution.py:38
  56.7 48.9 %reduce-scatter.2.cloned.1.call-start = ((), (), s32[]{:S(2)}) async-start(), calls=%async_computation.4 | async-start | bytes 147456 | tf_op jit(solution)/shard_map/reduce_scatter | solution.py:78
  61.6 1.6 %copy-start.1 = (bf16[2,128,4096]{2,1,0:T(8,128)(2,1)S(1)}, bf16[2,128,4096]{2,1,0:T(8,128)(2,1)}, u32[]{:S(2)}) copy-start(bf16[2,128,4096]{2,1,0:T(8,128)(2,1)} %param.15) | copy-start | bytes 6291460
  93.2 6.1 %copy-start.3 = (f32[16,4]{0,1:T(4,128)S(1)}, f32[16,4]{0,1:T(4,128)}, u32[]{:S(2)}) copy-start(f32[16,4]{0,1:T(4,128)} %param.13) | copy-start | bytes 772
  96.1 9.4 %all-to-all-start.2 = ((bf16[4,2,13,512]{3,1,2,0:T(2,128)(2,1)}), bf16[4,2,13,512]{3,1,2,0:T(2,128)(2,1)S(1)}, u32[]{:S(2)}, u32[]{:S(2)}) async-start(bf16[4,2,13,512]{3,1,2,0:T(2,128)(2,1)} %copy.51), calls=%async_computation.2 | async-start | bytes 212992 | tf_op jit(solution)/shard_map/all_to_all | solution.py:81
Sparse Core Ops, SparseCore 0:
  61.7 33.0 reduce-scatter.1
where the time goes:
time: 115 us; the launch traced here: 114 us
  blocking collectives  33.8 us (29%)
  waiting for transfers between devices  21.8 us (19%)
  local copies, waits for them, and re-layouts  17.5 us (15%)
  between operations  13.5 us (12%)
  starting transfers between devices  12.6 us (11%)
  matrix products  12.1 us (11%)
  other arithmetic  2.59 us (2%)
    all_gather x1, blocking collectives, per_device(): inner_whole = lax.all_gather(inner_vals, 'tp', axis=3, tiled=True)  22.9 us
    all_to_all x1, waiting for transfers between devices, per_device(): lax.all_to_all(packed, 'ep', split_axis=0, concat_axis=0, tiled=True)  15.8 us
    all_gather x1, blocking collectives, per_device(): gathered = lax.all_gather(hidden, 'tp', axis=1, tiled=True)  10.9 us
    unnamed x9, local copies, waits for them, and re-layouts  6.96 us
    all_to_all x1, local copies, waits for them, and re-layouts, per_device(): lax.all_to_all(down_weight, 'tp', split_axis=2, concat_axis=1, tiled=True)  6.15 us
    all_to_all x1, waiting for transfers between devices, per_device(): lax.all_to_all(answers, 'ep', split_axis=0, concat_axis=0, tiled=True)  5.96 us
    all_to_all x1, starting transfers between devices, per_device(): lax.all_to_all(packed, 'ep', split_axis=0, concat_axis=0, tiled=True)  4.87 us
    all_to_all x1, starting transfers between devices, per_device(): lax.all_to_all(down_weight, 'tp', split_axis=2, concat_axis=1, tiled=True)  4.34 us
  transfers between devices with their start and end apart: 4, of which 2 were waited for; matrix products, arithmetic and copies ran while one was open for 19% of the time, Pallas kernels for 0%

commit v1 on v0

--- a/solution.py
+++ b/solution.py
@@ -36,7 +36,13 @@
 ):
     width_group = lax.axis_size("tp")
     down_local = lax.all_to_all(down_weight, "tp", split_axis=2, concat_axis=1, tiled=True)
-    gathered = lax.all_gather(hidden, "tp", axis=1, tiled=True)
+    devices = lax.axis_size("tp")
+    block, blocks = (hidden, [hidden])
+    for _ in range(devices - 1):
+        block = lax.ppermute(block, "tp", [(i, (i + 1) % devices) for i in range(devices)])
+        blocks.insert(0, block)
+    line = jnp.concatenate(blocks, axis=1)
+    gathered = jnp.roll(line, (lax.axis_index("tp") + 1) * hidden.shape[1], axis=1)
     normed = norm_rows(gathered, norm_gain)
     tok_rows, top_count = routes.shape
     local_experts = gate_weight.shape[0]

time: 115 us -> 130 us (1.13)
  waiting for transfers between devices: 21.8 us -> 45.1 us
  blocking collectives: 33.8 us -> 22.9 us
  local copies, waits for them, and re-layouts: 17.5 us -> 19 us
    ppermute x0 -> x7, waiting for transfers between devices: none -> 26.5 us  [per_device(): lax.ppermute(block, 'tp', [(i, (i + 1) % devices) for i in range(devices)])]
    all_gather x1 -> x0, blocking collectives: 10.9 us -> none  [per_device(): gathered = lax.all_gather(hidden, 'tp', axis=1, tiled=True)]
    all_to_all x1, waiting for transfers between devices: 15.8 us -> 12.6 us  [per_device(): lax.all_to_all(packed, 'ep', split_axis=0, concat_axis=0, tiled=True)]
    unnamed x9 -> x24, local copies, waits for them, and re-layouts: 6.96 us -> 7.72 us
  transfers between devices with their start and end apart: 4 -> 11, of which waited for: 2 -> 9; matrix products, arithmetic and copies ran while one was open for 19% -> 19% of each run, Pallas kernels for 0% -> 0%
where the time goes in v1:
time: 130 us; the launch traced here: 129 us
  waiting for transfers between devices  45.1 us (35%)
  blocking collectives  22.9 us (18%)
  local copies, waits for them, and re-layouts  19 us (15%)
  starting transfers between devices  13.8 us (11%)
  between operations  13.6 us (10%)
  matrix products  12.1 us (9%)
  other arithmetic  2.43 us (2%)
    ppermute x7, waiting for transfers between devices, per_device(): lax.ppermute(block, 'tp', [(i, (i + 1) % devices) for i in range(devices)])  26.5 us
    all_gather x1, blocking collectives, per_device(): inner_whole = lax.all_gather(inner_vals, 'tp', axis=3, tiled=True)  22.9 us
    all_to_all x1, waiting for transfers between devices, per_device(): lax.all_to_all(packed, 'ep', split_axis=0, concat_axis=0, tiled=True)  12.6 us
    unnamed x24, local copies, waits for them, and re-layouts  7.72 us
    all_to_all x1, local copies, waits for them, and re-layouts, per_device(): lax.all_to_all(down_weight, 'tp', split_axis=2, concat_axis=1, tiled=True)  6.15 us
    all_to_all x1, waiting for transfers between devices, per_device(): lax.all_to_all(answers, 'ep', split_axis=0, concat_axis=0, tiled=True)  5.96 us
    all_to_all x1, starting transfers between devices, per_device(): lax.all_to_all(packed, 'ep', split_axis=0, concat_axis=0, tiled=True)  5.63 us
    all_to_all x1, starting transfers between devices, per_device(): lax.all_to_all(down_weight, 'tp', split_axis=2, concat_axis=1, tiled=True)  4.34 us
  transfers between devices with their start and end apart: 11, of which 9 were waited for; matrix products, arithmetic and copies ran while one was open for 19% of the time, Pallas kernels for 0%

profile of v1, /device:TPU:0, one launch (start us, length us, event | category | flops | bytes accessed | tf_op | source)
XLA Modules:
  0.0 128.9 jit_solution(14661916100457475905)
XLA Ops:
  6.5 0.5 collective-permute-start
  7.0 4.5 %collective-permute-done = bf16[16,512]{1,0:T(8,128)(2,1)S(1)} collective-permute-done((bf16[16,512]{1,0:T(8,128)(2,1)}, bf16[16,512]{1,0:T(8,128)(2,1)S(1)}, u32[]{:S(2)}, u32[]{:S(2)}) %collective-permute-start) | collective-permute-done | bytes 16416 | tf_op jit(solution)/shard_map/ppermute | solution.py:42
  11.5 4.1 %collective-permute-done.1 = bf16[16,512]{1,0:T(8,128)(2,1)S(1)} collective-permute-done((bf16[16,512]{1,0:T(8,128)(2,1)S(1)}, bf16[16,512]{1,0:T(8,128)(2,1)S(1)}, u32[]{:S(2)}, u32[]{:S(2)}) %collective-permute-start.1) | collective-permute-done | bytes 16416 | tf_op jit(solution)/shard_map/ppermute | solution.py:42
  15.6 4.1 %collective-permute-done.2 = bf16[16,512]{1,0:T(8,128)(2,1)S(1)} collective-permute-done((bf16[16,512]{1,0:T(8,128)(2,1)S(1)}, bf16[16,512]{1,0:T(8,128)(2,1)S(1)}, u32[]{:S(2)}, u32[]{:S(2)}) %collective-permute-start.2) | collective-permute-done | bytes 16416 | tf_op jit(solution)/shard_map/ppermute | solution.py:42
  19.7 0.7 convert_reduce_fusion
  20.5 3.2 %collective-permute-done.3 = bf16[16,512]{1,0:T(8,128)(2,1)S(1)} collective-permute-done((bf16[16,512]{1,0:T(8,128)(2,1)S(1)}, bf16[16,512]{1,0:T(8,128)(2,1)S(1)}, u32[]{:S(2)}, u32[]{:S(2)}) %collective-permute-start.3) | collective-permute-done | bytes 16416 | tf_op jit(solution)/shard_map/ppermute | solution.py:42
  23.7 0.7 select_reduce_fusion.1
  24.4 3.4 %collective-permute-done.4 = bf16[16,512]{1,0:T(8,128)(2,1)S(1)} collective-permute-done((bf16[16,512]{1,0:T(8,128)(2,1)S(1)}, bf16[16,512]{1,0:T(8,128)(2,1)S(1)}, u32[]{:S(2)}, u32[]{:S(2)}) %collective-permute-start.4) | collective-permute-done | bytes 16416 | tf_op jit(solution)/shard_map/ppermute | solution.py:42
  27.8 0.7 multiply_add_fusion
  28.5 3.4 %collective-permute-done.5 = bf16[16,512]{1,0:T(8,128)(2,1)S(1)} collective-permute-done((bf16[16,512]{1,0:T(8,128)(2,1)S(1)}, bf16[16,512]{1,0:T(8,128)(2,1)S(1)}, u32[]{:S(2)}, u32[]{:S(2)}) %collective-permute-start.5) | collective-permute-done | bytes 16416 | tf_op jit(solution)/shard_map/ppermute | solution.py:42
  32.0 4.0 %collective-permute-done.6 = bf16[16,512]{1,0:T(8,128)(2,1)S(1)} collective-permute-done((bf16[16,512]{1,0:T(8,128)(2,1)S(1)}, bf16[16,512]{1,0:T(8,128)(2,1)S(1)}, u32[]{:S(2)}, u32[]{:S(2)}) %collective-permute-start.6) | collective-permute-done | bytes 16416 | tf_op jit(solution)/shard_map/ppermute | solution.py:42
  36.0 0.7 constant_dynamic-update-slice_fusion.8
  36.7 0.7 constant_dynamic-update-slice_fusion
  37.6 2.1 %convolution_convert_fusion = bf16[104,4096]{1,0:T(8,128)(2,1)} fusion(bf16[104,16]{0,1:T(8,128)(2,1)S(1)} %fusion.33, f32[4096]{0:T(1024)} %param.11, f32[16]{0:T(128)S(1)} %add_rsqrt_fusion, bf16[16,8192]{1,0:T(8,128)(2,1)S(1)} %constant_dynamic-update-slice_fusion, s32[]{:T(128)S(6)} %select_n.19), kind=kOutput, calls=%fused_computation | convolution fusion | flops 14319616 | bytes 1004036 | tf_op jit(solution)/shard_map/dot_general | solution.py:60
  39.7 1.4 %reshape.33 = bf16[4,2,13,4096]{3,2,1,0:T(8,128)(2,1)S(1)} reshape(bf16[104,4096]{1,0:T(8,128)(2,1)} %convolution_convert_fusion) | data formatting | bytes 1703936 | tf_op jit(solution)/shard_map/reshape | solution.py:61
  41.1 1.8 %copy.43 = bf16[4,2,13,4096]{3,1,2,0:T(2,128)(2,1)} copy(bf16[4,2,13,4096]{3,2,1,0:T(8,128)(2,1)S(1)} %reshape.33) | data formatting | bytes 1703936 | tf_op jit(solution)/shard_map/reshape | solution.py:61
  43.0 5.6 %all-to-all-start = ((bf16[4,2,13,4096]{3,1,2,0:T(2,128)(2,1)}), bf16[4,2,13,4096]{3,1,2,0:T(2,128)(2,1)S(1)}, u32[]{:S(2)}, u32[]{:S(2)}) async-start(bf16[4,2,13,4096]{3,1,2,0:T(2,128)(2,1)} %copy.43), calls=%async_computation | async-start | bytes 1703936 | tf_op jit(solution)/shard_map/all_to_all | solution.py:62
  48.6 6.2 %copy.47 = bf16[2,128,4096]{1,0,2:T(2,128)(2,1)} copy(bf16[2,128,4096]{2,1,0:T(8,128)(2,1)} %param.16) | data formatting | bytes 4194304 | tf_op args[6]
  54.8 12.6 %all-to-all-done = bf16[4,2,13,4096]{3,1,2,0:T(2,128)(2,1)S(1)} async-done(((bf16[4,2,13,4096]{3,1,2,0:T(2,128)(2,1)}), bf16[4,2,13,4096]{3,1,2,0:T(2,128)(2,1)S(1)}, u32[]{:S(2)}, u32[]{:S(2)}) %all-to-all-start) | async-done | bytes 852000 | tf_op jit(solution)/shard_map/all_to_all | solution.py:62
  67.4 4.3 %all-to-all-start.1 = ((bf16[2,128,4096]{1,0,2:T(2,128)(2,1)}), bf16[2,128,4096]{1,0,2:T(2,128)(2,1)}, u32[]{:S(2)}, u32[]{:S(2)}) async-start(bf16[2,128,4096]{1,0,2:T(2,128)(2,1)} %copy.47), calls=%async_computation.1 | async-start | bytes 4194304 | tf_op jit(solution)/shard_map/all_to_all | solution.py:38
  71.8 1.6 %fusion.43 = f32[16,128]{1,0:T(8,128)S(1)} fusion(bf16[128,4096]{1,0:T(8,128)(2,1)} %param.17, f32[4096]{0:T(1024)S(1)} %copy-done.2, f32[16]{0:T(128)S(1)} %add_rsqrt_fusion, bf16[16,8192]{1,0:T(8,128)(2,1)S(1)} %constant_dynamic-update-slice_fusion, s32[]{:T(128)S(6)} %select_n.19), kind=kOutput, calls=%fused_computation.59 | convolution fusion | flops 17039360 | bytes 1204740 | tf_op jit(solution)/shard_map/dot_general | solution.py:69
  73.4 3.1 %convolution_convert_fusion.1 = bf16[16,4096]{1,0:T(8,128)(2,1)} fusion(bf16[128,4096]{1,0:T(8,128)(2,1)} %param.19, bf16[128,4096]{1,0:T(8,128)(2,1)} %param.18, f32[16,128]{1,0:T(8,128)S(1)} %fusion.43, f32[4096]{0:T(1024)S(1)} %copy-done.2, f32[16]{0:T(128)S(1)} %add_rsqrt_fusion, bf16[16,8192]{1,0:T(8,128)(2,1)S(1)} %constant_dynamic-update-slice_fusion, ...), kind=kOutput, calls=%fused_computation.1 | convolution fusion | flops 33894400 | bytes 2384388 | tf_op jit(solution)/shard_map/dot_general | solution.py:72
  76.6 0.8 fusion.12
  77.5 0.7 copy-done.1
  78.2 0.9 fusion.21
  79.1 22.9 %all_gather.3 = bf16[4,2,13,1024]{3,2,0,1:T(8,128)(2,1)S(1)} all-gather(bf16[4,2,13,128]{3,2,0,1:T(8,128)(2,1)S(1)} %fusion.21), channel_id=1, replica_groups=mesh['ep'=4,'tp'=8] {'tp'}, dimensions={3}, use_global_device_ids=true | all-gather | bytes 239616 | tf_op jit(solution)/shard_map/all_gather | solution.py:75
  102.2 6.2 %copy.49 = bf16[2,128,8,512]{3,1,2,0:T(8,128)(2,1)} copy(bf16[2,128,8,512]{1,0,3,2:T(2,128)(2,1)} %bitcast.6) | data formatting | bytes 4194304 | tf_op jit(solution)/shard_map/all_to_all | solution.py:38
  108.3 2.1 %fusion.9 = bf16[2,4,13,512]{3,2,1,0:T(8,128)(2,1)S(1)} fusion(bf16[2,128,8,512]{3,1,2,0:T(8,128)(2,1)} %copy.49, bf16[4,2,13,8,128]{4,3,2,0,1:T(8,128)(2,1)S(1)} %reshape.39), kind=kOutput, calls=%fused_computation.9 | convolution fusion | flops 109850624 | bytes 2416640 | tf_op jit(solution)/shard_map/secpf,epfd->secpd/dot_general | solution.py:80
  110.4 0.8 copy.51
  111.1 3.3 %all-to-all-start.2 = ((bf16[4,2,13,512]{3,1,2,0:T(2,128)(2,1)}), bf16[4,2,13,512]{3,1,2,0:T(2,128)(2,1)S(1)}, u32[]{:S(2)}, u32[]{:S(2)}) async-start(bf16[4,2,13,512]{3,1,2,0:T(2,128)(2,1)} %copy.51), calls=%async_computation.2 | async-start | bytes 212992 | tf_op jit(solution)/shard_map/all_to_all | solution.py:87
  114.5 6.0 %all-to-all-done.2 = bf16[4,2,13,512]{3,1,2,0:T(2,128)(2,1)S(1)} async-done(((bf16[4,2,13,512]{3,1,2,0:T(2,128)(2,1)}), bf16[4,2,13,512]{3,1,2,0:T(2,128)(2,1)S(1)}, u32[]{:S(2)}, u32[]{:S(2)}) %all-to-all-start.2) | async-done | bytes 106528 | tf_op jit(solution)/shard_map/all_to_all | solution.py:87
  120.6 1.5 %fusion.24 = bf16[16,512]{1,0:T(8,128)(2,1)} fusion(f32[16,104]{1,0:T(8,128)S(1)} %select_reduce_fusion, bf16[104,512]{1,0:T(8,128)(2,1)S(1)} %reshape.35, bf16[16,512]{1,0:T(8,128)(2,1)} %reduce-scatter.2.cloned.1.call-done), kind=kOutput, calls=%fused_computation.15 | convolution fusion | flops 10248192 | bytes 145920 | tf_op jit(solution)/shard_map/dot_general | solution.py:89
  (42 shorter events, 0.9 us)
Async XLA Ops:
  6.5 70.1 %copy-start = (bf16[2,128,4096]{2,1,0:T(8,128)(2,1)S(1)}, bf16[2,128,4096]{2,1,0:T(8,128)(2,1)}, u32[]{:S(2)}) copy-start(bf16[2,128,4096]{2,1,0:T(8,128)(2,1)} %param.14) | copy-start | bytes 6291460
  6.5 5.0 %collective-permute-start = (bf16[16,512]{1,0:T(8,128)(2,1)}, bf16[16,512]{1,0:T(8,128)(2,1)S(1)}, u32[]{:S(2)}, u32[]{:S(2)}) collective-permute-start(bf16[16,512]{1,0:T(8,128)(2,1)} %param.10), channel_id=1, source_target_pairs={{0,1},{1,2},{2,3},{3,4},{4,5},{5,6},{6,7},{7,0},{8,9},{9,10},{10,1... | collective-permute-start | bytes 49160 | tf_op jit(solution)/shard_map/ppermute | solution.py:42
  11.5 4.1 %collective-permute-start.1 = (bf16[16,512]{1,0:T(8,128)(2,1)S(1)}, bf16[16,512]{1,0:T(8,128)(2,1)S(1)}, u32[]{:S(2)}, u32[]{:S(2)}) collective-permute-start(bf16[16,512]{1,0:T(8,128)(2,1)S(1)} %collective-permute-done), channel_id=1, source_target_pairs={{0,1},{1,2},{2,3},{3,4},{4,5},{5,6},{6,7},{7,0},{8,9},{9,10},{10,1... | collective-permute-start | bytes 49160 | tf_op jit(solution)/shard_map/ppermute | solution.py:42
  15.6 4.1 %collective-permute-start.2 = (bf16[16,512]{1,0:T(8,128)(2,1)S(1)}, bf16[16,512]{1,0:T(8,128)(2,1)S(1)}, u32[]{:S(2)}, u32[]{:S(2)}) collective-permute-start(bf16[16,512]{1,0:T(8,128)(2,1)S(1)} %collective-permute-done.1), channel_id=1, source_target_pairs={{0,1},{1,2},{2,3},{3,4},{4,5},{5,6},{6,7},{7,0},{8,9},{9,10},{10,1... | collective-permute-start | bytes 49160 | tf_op jit(solution)/shard_map/ppermute | solution.py:42
  19.7 4.1 %collective-permute-start.3 = (bf16[16,512]{1,0:T(8,128)(2,1)S(1)}, bf16[16,512]{1,0:T(8,128)(2,1)S(1)}, u32[]{:S(2)}, u32[]{:S(2)}) collective-permute-start(bf16[16,512]{1,0:T(8,128)(2,1)S(1)} %collective-permute-done.2), channel_id=1, source_target_pairs={{0,1},{1,2},{2,3},{3,4},{4,5},{5,6},{6,7},{7,0},{8,9},{9,10},{10,1... | collective-permute-start | bytes 49160 | tf_op jit(solution)/shard_map/ppermute | solution.py:42
  23.7 4.1 %collective-permute-start.4 = (bf16[16,512]{1,0:T(8,128)(2,1)S(1)}, bf16[16,512]{1,0:T(8,128)(2,1)S(1)}, u32[]{:S(2)}, u32[]{:S(2)}) collective-permute-start(bf16[16,512]{1,0:T(8,128)(2,1)S(1)} %collective-permute-done.3), channel_id=1, source_target_pairs={{0,1},{1,2},{2,3},{3,4},{4,5},{5,6},{6,7},{7,0},{8,9},{9,10},{10,1... | collective-permute-start | bytes 49160 | tf_op jit(solution)/shard_map/ppermute | solution.py:42
  27.8 4.1 %collective-permute-start.5 = (bf16[16,512]{1,0:T(8,128)(2,1)S(1)}, bf16[16,512]{1,0:T(8,128)(2,1)S(1)}, u32[]{:S(2)}, u32[]{:S(2)}) collective-permute-start(bf16[16,512]{1,0:T(8,128)(2,1)S(1)} %collective-permute-done.4), channel_id=1, source_target_pairs={{0,1},{1,2},{2,3},{3,4},{4,5},{5,6},{6,7},{7,0},{8,9},{9,10},{10,1... | collective-permute-start | bytes 49160 | tf_op jit(solution)/shard_map/ppermute | solution.py:42
  31.9 4.1 %collective-permute-start.6 = (bf16[16,512]{1,0:T(8,128)(2,1)S(1)}, bf16[16,512]{1,0:T(8,128)(2,1)S(1)}, u32[]{:S(2)}, u32[]{:S(2)}) collective-permute-start(bf16[16,512]{1,0:T(8,128)(2,1)S(1)} %collective-permute-done.5), channel_id=1, source_target_pairs={{0,1},{1,2},{2,3},{3,4},{4,5},{5,6},{6,7},{7,0},{8,9},{9,10},{10,1... | collective-permute-start | bytes 49160 | tf_op jit(solution)/shard_map/ppermute | solution.py:42
  43.0 24.4 %all-to-all-start = ((bf16[4,2,13,4096]{3,1,2,0:T(2,128)(2,1)}), bf16[4,2,13,4096]{3,1,2,0:T(2,128)(2,1)S(1)}, u32[]{:S(2)}, u32[]{:S(2)}) async-start(bf16[4,2,13,4096]{3,1,2,0:T(2,128)(2,1)} %copy.43), calls=%async_computation | async-start | bytes 1703936 | tf_op jit(solution)/shard_map/all_to_all | solution.py:62
  54.8 17.0 %copy-start.2 = (f32[4096]{0:T(1024)S(1)}, f32[4096]{0:T(1024)}, u32[]{:S(2)}) copy-start(f32[4096]{0:T(1024)} %param.11) | copy-start | bytes 49156
  67.4 34.8 %all-to-all-start.1 = ((bf16[2,128,4096]{1,0,2:T(2,128)(2,1)}), bf16[2,128,4096]{1,0,2:T(2,128)(2,1)}, u32[]{:S(2)}, u32[]{:S(2)}) async-start(bf16[2,128,4096]{1,0,2:T(2,128)(2,1)} %copy.47), calls=%async_computation.1 | async-start | bytes 4194304 | tf_op jit(solution)/shard_map/all_to_all | solution.py:38
  71.7 48.9 %reduce-scatter.2.cloned.1.call-start = ((), (), s32[]{:S(2)}) async-start(), calls=%async_computation.4 | async-start | bytes 147456 | tf_op jit(solution)/shard_map/reduce_scatter | solution.py:84
  76.6 1.6 %copy-start.1 = (bf16[2,128,4096]{2,1,0:T(8,128)(2,1)S(1)}, bf16[2,128,4096]{2,1,0:T(8,128)(2,1)}, u32[]{:S(2)}) copy-start(bf16[2,128,4096]{2,1,0:T(8,128)(2,1)} %param.15) | copy-start | bytes 6291460
  108.3 6.1 %copy-start.3 = (f32[16,4]{0,1:T(4,128)S(1)}, f32[16,4]{0,1:T(4,128)}, u32[]{:S(2)}) copy-start(f32[16,4]{0,1:T(4,128)} %param.13) | copy-start | bytes 772
  111.1 9.4 %all-to-all-start.2 = ((bf16[4,2,13,512]{3,1,2,0:T(2,128)(2,1)}), bf16[4,2,13,512]{3,1,2,0:T(2,128)(2,1)S(1)}, u32[]{:S(2)}, u32[]{:S(2)}) async-start(bf16[4,2,13,512]{3,1,2,0:T(2,128)(2,1)} %copy.51), calls=%async_computation.2 | async-start | bytes 212992 | tf_op jit(solution)/shard_map/all_to_all | solution.py:87
Sparse Core Ops, SparseCore 0:
  76.7 33.0 reduce-scatter.1
